TPU v7x, 32 devices: a whole 2x2x4 slice. The times are simulated.
32 devices in a mesh: sp: 8 (over z, y), dp: 4 (over x, core).
Axes of the slice: x: 2, y: 2, z: 4, core: 2. Of those that a mesh axis runs over, the one named last changes fastest.
Arguments:
- skip_connection_stream: bfloat16 [4, 1024, 2048], P('dp', 'sp'), may hold values from -6 to 6
- emitted_valve_unscaled: bfloat16 [4, 1024, 1024], P('dp', 'sp'), may hold values from -6 to 6
- channel_source_mapped: bfloat16 [4, 1024, 1024], P('dp', 'sp'), may hold values from -6 to 6
- hidden_source_mapped: bfloat16 [4, 1024, 256], P('dp', 'sp'), may hold values from -6 to 6
- probe_mapped_values: bfloat16 [4, 1024, 256], P('dp', 'sp'), may hold values from -6 to 6
- increment_premapped: float32 [4, 1024, 16], P('dp', None, 'sp'), may hold values from -6 to 6
- extra_log_fading: float32 [4, 1024, 16], P('dp', None, 'sp'), may hold values from -2 to 0
- channel_fading_speed: float32 [16], replicated, may hold values from 0 to 1, as said below
- channel_source_kernel: float32 [4, 1024], replicated, may hold values from -3 to 3
- hidden_source_kernel: float32 [4, 256], replicated, may hold values from -3 to 3
- probe_kernel_coefficients: float32 [4, 256], replicated, may hold values from -3 to 3
- cluster_scaling_factor: float32 [1024], replicated, may hold values from 0.1 to 1.9
- emitted_mapping_matrix: bfloat16 [1024, 2048], replicated, may hold values from -0.1875 to 0.1875
- standardize_scaling: float32 [2048], replicated, may hold values from 0.1 to 1.9
- standardize_offset: float32 [2048], replicated, may hold values from -2 to 2
- chosen_specialist_ids: int32 [4, 1024, 2], P('dp', 'sp'), may hold values from 0 to 7, all different within a row; in each aligned block of 128 rows (0 to 127, 128 to 255, ..., all dimensions but the last counted through in order) at most 48 rows name the same one
- specialist_mixing_shares: float32 [4, 1024, 2], P('dp', 'sp'), may hold values from 0.2 to 1
- specialist_gating_matrices: bfloat16 [8, 2048, 5120], P('sp', None, 'dp'), may hold values from -0.125 to 0.125
- raising_matrices: bfloat16 [8, 2048, 5120], P('sp', None, 'dp'), may hold values from -0.125 to 0.125
- lowering_matrices: bfloat16 [8, 5120, 2048], P('sp', 'dp'), may hold values from -0.078125 to 0.078125
Outputs:
- layer_out: bfloat16 [4, 1024, 2048], P('dp', 'sp')
Inputs may be any that keep to these rules, and one draw needn't show every extreme that they name: `chosen_specialist_ids`: each row names two different experts. The rows of one device name no expert more than 48 times, a bound that some block reaches. `channel_fading_speed`: Positive.
All inputs are finite; a program needn't handle non-finite values.
Results may differ from a plain program's by a relative error of at most 0.015.
Values may be sent and summed in bfloat16 or wider, within the bound.
No kernel may reach another device: no remote copies, remote signals or barrier semaphores. Data moves between devices by JAX's collectives and lax.ppermute only.
A program may use at most 128 MiB of HBM per device.

v0:
```python
import jax
import jax.numpy as jnp
from jax import lax
from jax.sharding import PartitionSpec as P

HEADS = 16
HEAD_DIM = 64
GROUPS = 4
STATE = 64
KERNEL = 4
BLK = 128


rms_eps = 1e-06
norm_eps = 1e-05


def causal_conv(series, tap_weights, rim_rows):
    padded = jnp.concatenate([rim_rows, series], axis=0).astype(jnp.float32)
    length = series.shape[0]
    running = jnp.zeros(series.shape, jnp.float32)
    for tap_index in range(tap_weights.shape[0]):
        running = running + tap_weights[tap_index] * lax.slice_in_dim(
            padded, tap_index, tap_index + length, axis=0
        )
    return jax.nn.silu(running).astype(jnp.bfloat16)


def ssd_blocks(x_conv, b_conv, c_conv, increment_delta, fading_exponent, init_state, block_len):
    length, head_count, head_width = x_conv.shape
    state_width = b_conv.shape[2]
    block_count = length // block_len
    x_block = x_conv.reshape(block_count, block_len, head_count, head_width)
    b_block = b_conv.reshape(block_count, block_len, head_count, state_width)
    c_block = c_conv.reshape(block_count, block_len, head_count, state_width)
    cumulative = jnp.cumsum(
        jnp.transpose(fading_exponent.reshape(block_count, block_len, head_count), (0, 2, 1)),
        axis=2,
    )
    step_heads = jnp.transpose(
        increment_delta.reshape(block_count, block_len, head_count), (0, 2, 1)
    )
    causal = jnp.arange(block_len)[:, None] >= jnp.arange(block_len)[None, :]
    within = jnp.exp(
        jnp.where(causal, cumulative[:, :, :, None] - cumulative[:, :, None, :], -jnp.inf)
    )
    scores = jnp.einsum("cthn,cshn->chts", c_block, b_block, preferred_element_type=jnp.float32)
    mixing = (scores * within * step_heads[:, :, None, :]).astype(jnp.bfloat16)
    diag_out = jnp.einsum("chts,cshp->cthp", mixing, x_block, preferred_element_type=jnp.float32)
    tail_decay = jnp.exp(cumulative[:, :, -1:] - cumulative) * step_heads
    scaled = (
        x_block.astype(jnp.float32) * jnp.transpose(tail_decay, (0, 2, 1))[:, :, :, None]
    ).astype(jnp.bfloat16)
    block_state = jnp.einsum("cshp,cshn->chpn", scaled, b_block, preferred_element_type=jnp.float32)
    totals = cumulative[:, :, -1]
    through = jnp.cumsum(totals, axis=0)
    before = through - totals
    earlier = jnp.arange(block_count)[:, None] > jnp.arange(block_count)[None, :]
    carry_weight = jnp.exp(
        jnp.where(earlier[:, :, None], before[:, None, :] - through[None, :, :], -jnp.inf)
    )
    entering = (
        jnp.einsum("cjh,jhpn->chpn", carry_weight, block_state, precision=lax.Precision.HIGHEST)
        + jnp.exp(before)[:, :, None, None] * init_state[None]
    )
    reach_decay = jnp.transpose(jnp.exp(cumulative), (0, 2, 1))
    carried_out = (
        jnp.einsum(
            "cthn,chpn->cthp",
            c_block.astype(jnp.float32),
            entering,
            precision=lax.Precision.HIGHEST,
        )
        * reach_decay[:, :, :, None]
    )
    outcome = (diag_out + carried_out).reshape(length, head_count, head_width)
    final_state = (
        jnp.einsum(
            "jh,jhpn->hpn",
            jnp.exp(through[-1][None, :] - through),
            block_state,
            precision=lax.Precision.HIGHEST,
        )
        + jnp.exp(through[-1])[:, None, None] * init_state
    )
    return (outcome, final_state, through[-1])


def per_device(
    skip_connection_stream,
    emitted_valve_unscaled,
    channel_source_mapped,
    hidden_source_mapped,
    probe_mapped_values,
    increment_premapped,
    extra_log_fading,
    channel_fading_speed,
    channel_source_kernel,
    hidden_source_kernel,
    probe_kernel_coefficients,
    cluster_scaling_factor,
    emitted_mapping_matrix,
    standardize_scaling,
    standardize_offset,
    chosen_specialist_ids,
    specialist_mixing_shares,
    specialist_gating_matrices,
    raising_matrices,
    lowering_matrices,
):
    sp_size = lax.axis_size("sp")
    sp_index = lax.axis_index("sp")
    tok_rows = skip_connection_stream.shape[1]
    model_width = skip_connection_stream.shape[2]
    inner_width = HEADS * HEAD_DIM
    per_group = HEADS // GROUPS
    paired = HEAD_DIM + 2 * STATE
    head_count = HEADS // sp_size
    first_head = sp_index * head_count
    x_heads = channel_source_mapped[0].reshape(tok_rows, HEADS, HEAD_DIM)
    b_heads = jnp.repeat(
        hidden_source_mapped[0].reshape(tok_rows, GROUPS, STATE), per_group, axis=1
    )
    c_heads = jnp.repeat(probe_mapped_values[0].reshape(tok_rows, GROUPS, STATE), per_group, axis=1)
    payload = jnp.concatenate([x_heads, b_heads, c_heads], axis=2)
    arrived = lax.all_to_all(payload, "sp", split_axis=1, concat_axis=0, tiled=True)
    taps_x = lax.dynamic_slice_in_dim(
        channel_source_kernel.reshape(KERNEL, HEADS, HEAD_DIM), first_head, head_count, 1
    )
    taps_b = lax.dynamic_slice_in_dim(
        jnp.repeat(hidden_source_kernel.reshape(KERNEL, GROUPS, STATE), per_group, axis=1),
        first_head,
        head_count,
        1,
    )
    taps_c = lax.dynamic_slice_in_dim(
        jnp.repeat(probe_kernel_coefficients.reshape(KERNEL, GROUPS, STATE), per_group, axis=1),
        first_head,
        head_count,
        1,
    )
    rim_rows = jnp.zeros((KERNEL - 1, head_count, paired), jnp.bfloat16)
    convolved = causal_conv(arrived, jnp.concatenate([taps_x, taps_b, taps_c], axis=2), rim_rows)
    increment_delta = jax.nn.softplus(increment_premapped[0])
    speeds_per_channel = lax.dynamic_slice_in_dim(channel_fading_speed, first_head, head_count, 0)
    fading_exponent = extra_log_fading[0] - speeds_per_channel[None, :] * increment_delta
    init_state = jnp.zeros((head_count, HEAD_DIM, STATE), jnp.float32)
    outcome, final_state, total_decay = ssd_blocks(
        convolved[:, :, :HEAD_DIM],
        convolved[:, :, HEAD_DIM : HEAD_DIM + STATE],
        convolved[:, :, HEAD_DIM + STATE :],
        increment_delta,
        fading_exponent,
        init_state,
        BLK,
    )
    returned_rows = lax.all_to_all(
        outcome.astype(jnp.bfloat16), "sp", split_axis=0, concat_axis=1, tiled=True
    )
    blending_outcome = returned_rows.reshape(tok_rows, inner_width)
    gated = blending_outcome.astype(jnp.float32) * jax.nn.silu(
        emitted_valve_unscaled[0].astype(jnp.float32)
    )
    grouped = gated.reshape(tok_rows, GROUPS, inner_width // GROUPS)
    grouped = grouped * lax.rsqrt(jnp.mean(grouped * grouped, axis=-1, keepdims=True) + rms_eps)
    group_normed = (
        grouped.reshape(tok_rows, inner_width) * cluster_scaling_factor[None, :]
    ).astype(jnp.bfloat16)
    pre_norm = skip_connection_stream[0].astype(jnp.float32) + jnp.dot(
        group_normed, emitted_mapping_matrix, preferred_element_type=jnp.float32
    )
    centre = jnp.mean(pre_norm, axis=-1, keepdims=True)
    variance = jnp.mean(jnp.square(pre_norm - centre), axis=-1, keepdims=True)
    normed = (
        (pre_norm - centre) * lax.rsqrt(variance + norm_eps) * standardize_scaling[None, :]
        + standardize_offset[None, :]
    ).astype(jnp.bfloat16)
    slot_cap = 3 * tok_rows // sp_size
    flat_ids = chosen_specialist_ids[0].reshape(-1)
    matched = (flat_ids[:, None] == jnp.arange(sp_size, dtype=jnp.int32)[None, :]).astype(jnp.int32)
    ranked = jnp.cumsum(matched, axis=0) - 1
    target = flat_ids * slot_cap + jnp.sum(matched * ranked, axis=1)
    placing = (jnp.arange(sp_size * slot_cap, dtype=jnp.int32)[:, None] == target[None, :]).astype(
        jnp.bfloat16
    )
    placing = jnp.sum(placing.reshape(sp_size * slot_cap, tok_rows, 2), axis=2)
    outgoing = (
        jnp.dot(placing, normed, preferred_element_type=jnp.float32)
        .astype(jnp.bfloat16)
        .reshape(sp_size, slot_cap, model_width)
    )
    arrived_rows = lax.all_gather(
        lax.all_to_all(outgoing, "sp", split_axis=0, concat_axis=0, tiled=True)[:, None],
        "dp",
        axis=1,
        tiled=True,
    )
    flattened = arrived_rows.reshape(-1, model_width)
    gate_val = jnp.dot(flattened, specialist_gating_matrices[0], preferred_element_type=jnp.float32)
    up_val = jnp.dot(flattened, raising_matrices[0], preferred_element_type=jnp.float32)
    hidden = (jax.nn.silu(gate_val) * up_val).astype(jnp.bfloat16)
    partial_value = jnp.dot(
        hidden, lowering_matrices[0], preferred_element_type=jnp.float32
    ).astype(jnp.bfloat16)
    partial_rows = (
        lax.optimization_barrier(partial_value).astype(jnp.float32).reshape(arrived_rows.shape)
    )
    summed = lax.psum_scatter(
        partial_rows.astype(jnp.bfloat16), "dp", scatter_dimension=1, tiled=True
    )
    item_count = partial_rows.shape[2]
    answer_rows = summed.reshape(sp_size, item_count, model_width)
    answered = lax.all_to_all(answer_rows, "sp", split_axis=0, concat_axis=0, tiled=True)
    picked = answered.reshape(sp_size * slot_cap, model_width)[target.reshape(tok_rows, 2)]
    routed_sum = jnp.sum(
        specialist_mixing_shares[0][:, :, None] * picked.astype(jnp.float32), axis=1
    )
    layer_out = (normed.astype(jnp.float32) + routed_sum).astype(jnp.bfloat16)
    return layer_out[None]


def solution(mesh):
    placed = (
        P("dp", "sp", None),
        P("dp", "sp", None),
        P("dp", "sp", None),
        P("dp", "sp", None),
        P("dp", "sp", None),
        P("dp", None, "sp"),
        P("dp", None, "sp"),
        P(),
        P(),
        P(),
        P(),
        P(),
        P(),
        P(),
        P(),
        P("dp", "sp", None),
        P("dp", "sp", None),
        P("sp", None, "dp"),
        P("sp", None, "dp"),
        P("sp", "dp", None),
    )
    return jax.shard_map(
        per_device, mesh=mesh, in_specs=placed, out_specs=P("dp", "sp", None), check_vma=False
    )
```

profile of v0, /device:TPU:0, one launch (start us, length us, event | category | flops | bytes accessed | tf_op | source)
XLA Modules:
  0.0 370.2 jit_solution(385357176187847751)
XLA Ops:
  6.6 1.0 copy.134
  7.6 1.0 copy.135
  8.6 1.1 copy.133
  9.8 0.9 pad_maximum_fusion
  10.7 7.3 %all-to-all-start = ((bf16[128,16,192]{0,2,1:T(8,128)(2,1)}), bf16[128,16,192]{0,2,1:T(8,128)(2,1)S(1)}, u32[]{:S(2)}, u32[]{:S(2)}) async-start(bf16[128,16,192]{0,2,1:T(8,128)(2,1)} %pad_maximum_fusion), calls=%async_computation | async-start | bytes 1572864 | tf_op jit(solution)/shard_map/all_to_all | solution.py:126
  21.2 17.0 %all-to-all-done = bf16[128,16,192]{0,2,1:T(8,128)(2,1)S(1)} async-done(((bf16[128,16,192]{0,2,1:T(8,128)(2,1)}), bf16[128,16,192]{0,2,1:T(8,128)(2,1)S(1)}, u32[]{:S(2)}, u32[]{:S(2)}) %all-to-all-start) | async-done | bytes 786464 | tf_op jit(solution)/shard_map/all_to_all | solution.py:126
  38.8 1.6 multiply_convert_fusion
  41.0 0.9 fusion.14
  43.6 1.1 reshape.249
  44.7 3.7 all-to-all-start.1
  48.8 8.7 %all-to-all-done.1 = bf16[8,2,8192]{2,1,0:T(2,128)(2,1)S(1)} async-done(((bf16[8,2,8192]{2,1,0:T(2,128)(2,1)}), bf16[8,2,8192]{2,1,0:T(2,128)(2,1)S(1)}, u32[]{:S(2)}, u32[]{:S(2)}) %all-to-all-start.1) | async-done | bytes 262176 | tf_op jit(solution)/shard_map/all_to_all | solution.py:157
  59.1 3.0 fusion.72
  63.1 40.2 %all_to_all.37 = bf16[8,48,2048]{2,1,0:T(8,128)(2,1)} all-to-all(bf16[8,48,2048]{2,1,0:T(8,128)(2,1)S(1)} %bitcast.198), channel_id=1, replica_groups=mesh['sp'=8,'dp'=4] {'sp'}, dimensions={0} | all-to-all | bytes 3145728 | tf_op jit(solution)/shard_map/all_to_all | solution.py:193
  103.5 45.2 %all-gather.3.cloned.1.call-done = bf16[8,192,2048]{2,1,0:T(8,128)(2,1)} async-done(((bf16[8,48,2048]{2,1,0:T(8,128)(2,1)}), bf16[8,192,2048]{2,1,0:T(8,128)(2,1)}) %all-gather.3.cloned.1.call-update) | async-done | bytes 6291472 | tf_op jit(solution)/shard_map/all_gather | solution.py:192
  148.8 13.8 %fusion.6 = f32[1536,1280]{1,0:T(8,128)} fusion(bf16[1536,2048]{1,0:T(8,128)(2,1)} %bitcast.220, bf16[1,2048,1280]{2,1,0:T(8,128)(2,1)} %param.37), kind=kOutput, calls=%fused_computation.7 | convolution fusion | flops 8053063680 | bytes 19398656 | tf_op jit(solution)/shard_map/dot_general | solution.py:199
  162.6 26.5 %fusion.2 = bf16[1536,2048]{1,0:T(8,128)(2,1)} fusion(bf16[1536,2048]{1,0:T(8,128)(2,1)} %bitcast.221, f32[1536,1280]{1,0:T(8,128)} %fusion.6, bf16[1,1280,2048]{2,1,0:T(8,128)(2,1)} %param.39, bf16[1,2048,1280]{2,1,0:T(8,128)(2,1)} %param.38), kind=kOutput, calls=%fused_computation.4 | convolution fusion | flops 16121069568 | bytes 30932992 | tf_op jit(solution)/shard_map/dot_general | solution.py:202
  190.4 118.5 %all-reduce.4.cloned.1.call-done = bf16[8,4,48,2048]{3,2,1,0:T(8,128)(2,1)} async-done(((bf16[8,4,48,2048]{3,2,1,0:T(8,128)(2,1)}), bf16[8,4,48,2048]{3,2,1,0:T(8,128)(2,1)}) %all-reduce.4.cloned.1.call-update) | async-done | bytes 6291472
  308.9 3.4 dynamic-slice_bitcast_fusion
  312.3 5.5 %all-to-all-start.3 = ((bf16[8,48,2048]{2,1,0:T(8,128)(2,1)}), bf16[8,48,2048]{2,1,0:T(8,128)(2,1)S(1)}, u32[]{:S(2)}, u32[]{:S(2)}) async-start(bf16[8,48,2048]{2,1,0:T(8,128)(2,1)} %dynamic-slice_bitcast_fusion), calls=%async_computation.3 | async-start | bytes 3145728 | tf_op jit(solution)/shard_map/all_to_all | solution.py:213
  318.2 36.2 %all-to-all-done.3 = bf16[8,48,2048]{2,1,0:T(8,128)(2,1)S(1)} async-done(((bf16[8,48,2048]{2,1,0:T(8,128)(2,1)}), bf16[8,48,2048]{2,1,0:T(8,128)(2,1)S(1)}, u32[]{:S(2)}, u32[]{:S(2)}) %all-to-all-start.3) | async-done | bytes 1572896 | tf_op jit(solution)/shard_map/all_to_all | solution.py:213
  354.4 2.3 gather_fusion
  356.8 2.4 reshape.242
  359.1 3.2 multiply_reduce_fusion
  362.3 1.1 fusion.21
  (102 shorter events, 10.7 us)
Async XLA Ops:
  6.5 11.5 %copy-start.13 = (f32[16]{0:T(128)S(1)}, f32[16]{0:T(128)}, u32[]{:S(2)}) copy-start(f32[16]{0:T(128)} %param.27) | copy-start | bytes 196
  6.5 11.6 %copy-start.4 = (f32[1,1024,2]{1,2,0:T(2,128)S(1)}, f32[1,1024,2]{1,2,0:T(2,128)}, u32[]{:S(2)}) copy-start(f32[1,1024,2]{1,2,0:T(2,128)} %param.25) | copy-start | bytes 24580
  6.5 11.6 %copy-start.6 = (f32[1,1024,2]{1,2,0:T(2,128)S(1)}, f32[1,1024,2]{1,2,0:T(2,128)}, u32[]{:S(2)}) copy-start(f32[1,1024,2]{1,2,0:T(2,128)} %param.26) | copy-start | bytes 24580
  6.5 12.7 %copy-start.11 = (s32[1,128,2]{1,2,0:T(2,128)S(1)}, s32[1,128,2]{1,2,0:T(2,128)}, u32[]{:S(2)}) copy-start(s32[1,128,2]{1,2,0:T(2,128)} %param.35) | copy-start | bytes 3076
  6.5 13.1 %copy-start.9 = (f32[4,256]{1,0:T(4,128)S(1)}, f32[4,256]{1,0:T(4,128)}, u32[]{:S(2)}) copy-start(f32[4,256]{1,0:T(4,128)} %param.29) | copy-start | bytes 12292
  6.5 13.2 %copy-start.10 = (f32[4,256]{1,0:T(4,128)S(1)}, f32[4,256]{1,0:T(4,128)}, u32[]{:S(2)}) copy-start(f32[4,256]{1,0:T(4,128)} %param.30) | copy-start | bytes 12292
  6.6 13.2 %copy-start.5 = (f32[4,1024]{1,0:T(4,128)S(1)}, f32[4,1024]{1,0:T(4,128)}, u32[]{:S(2)}) copy-start(f32[4,1024]{1,0:T(4,128)} %param.28) | copy-start | bytes 49156
  6.6 13.3 %copy-start.1 = (bf16[1,128,1024]{2,1,0:T(8,128)(2,1)S(1)}, bf16[1,128,1024]{2,1,0:T(8,128)(2,1)}, u32[]{:S(2)}) copy-start(bf16[1,128,1024]{2,1,0:T(8,128)(2,1)} %param.21) | copy-start | bytes 786436
  10.7 27.5 %all-to-all-start = ((bf16[128,16,192]{0,2,1:T(8,128)(2,1)}), bf16[128,16,192]{0,2,1:T(8,128)(2,1)S(1)}, u32[]{:S(2)}, u32[]{:S(2)}) async-start(bf16[128,16,192]{0,2,1:T(8,128)(2,1)} %pad_maximum_fusion), calls=%async_computation | async-start | bytes 1572864 | tf_op jit(solution)/shard_map/all_to_all | solution.py:126
  21.0 19.4 %copy-start.7 = (s32[8,3]{0,1:T(4,128)}, s32[8,3]{0,1:T(4,128)S(1)}, u32[]{:S(2)}) copy-start(s32[8,3]{0,1:T(4,128)S(1)} %reduce-window.9) | copy-start | bytes 292
  41.0 7.4 %slice-start = ((s32[8,3]{0,1:T(4,128)}), s32[8,2]{0,1:T(2,128)S(1)}, s32[]{:S(2)}) async-start(s32[8,3]{0,1:T(4,128)} %copy-done.7), calls=%async_computation.6 | async-start | bytes 2048 | tf_op jit(solution)/shard_map/slice.1
  43.1 15.7 %copy-start.8 = (f32[1024]{0:T(1024)S(1)}, f32[1024]{0:T(1024)}, u32[]{:S(2)}) copy-start(f32[1024]{0:T(1024)} %param.31) | copy-start | bytes 12292
  44.7 14.5 %copy-start = (bf16[1,128,2048]{2,1,0:T(8,128)(2,1)S(1)}, bf16[1,128,2048]{2,1,0:T(8,128)(2,1)}, u32[]{:S(2)}) copy-start(bf16[1,128,2048]{2,1,0:T(8,128)(2,1)} %param.20) | copy-start | bytes 1572868
  44.7 12.8 %all-to-all-start.1 = ((bf16[8,2,8192]{2,1,0:T(2,128)(2,1)}), bf16[8,2,8192]{2,1,0:T(2,128)(2,1)S(1)}, u32[]{:S(2)}, u32[]{:S(2)}) async-start(bf16[8,2,8192]{2,1,0:T(2,128)(2,1)} %reshape.249), calls=%async_computation.1 | async-start | bytes 524288 | tf_op jit(solution)/shard_map/all_to_all | solution.py:157
  48.4 100.4 %all-gather.3.cloned.1.call-start = ((), (), s32[]{:S(2)}) async-start(), calls=%async_computation.4 | async-start | bytes 7864320 | tf_op jit(solution)/shard_map/all_gather | solution.py:192
  58.9 3.5 copy-start.2
  58.9 3.5 copy-start.3
  103.3 205.6 %all-reduce.4.cloned.1.call-start = ((), (), s32[]{:S(2)}) async-start(), calls=%async_computation.5 | async-start | bytes 12582912
  189.1 0.7 copy-start.14
  189.2 128.9 %copy-start.12 = (f32[1,128,2]{1,2,0:T(2,128)S(1)}, f32[1,128,2]{1,2,0:T(2,128)}, u32[]{:S(2)}) copy-start(f32[1,128,2]{1,2,0:T(2,128)} %param.36) | copy-start | bytes 3076
  312.3 42.1 %all-to-all-start.3 = ((bf16[8,48,2048]{2,1,0:T(8,128)(2,1)}), bf16[8,48,2048]{2,1,0:T(8,128)(2,1)S(1)}, u32[]{:S(2)}, u32[]{:S(2)}) async-start(bf16[8,48,2048]{2,1,0:T(8,128)(2,1)} %dynamic-slice_bitcast_fusion), calls=%async_computation.3 | async-start | bytes 3145728 | tf_op jit(solution)/shard_map/all_to_all | solution.py:213
Sparse Core Ops, SparseCore 0:
  103.4 45.3 all-gather.2
  189.3 119.5 all-reduce.3
where the time goes:
time: 371 us; the launch traced here: 370 us
  waiting for transfers between devices  226 us (61%)
  matrix products  46.4 us (13%)
  blocking collectives  40.2 us (11%)
  local copies, waits for them, and re-layouts  17.3 us (5%)
  starting transfers between devices  16.8 us (5%)
  between operations  13.9 us (4%)
  other arithmetic  9.97 us (3%)
    unnamed x3, waiting for transfers between devices  119 us
    all_gather x1, waiting for transfers between devices, per_device(): lax.all_gather(lax.all_to_all(outgoing, 'sp', split_axis=0, concat_axis=0...  45.2 us
    all_to_all x1, blocking collectives, per_device(): lax.all_to_all(outgoing, 'sp', split_axis=0, concat_axis=0, tiled=True)  40.2 us
    all_to_all x1, waiting for transfers between devices, per_device(): lax.all_to_all(answer_rows, 'sp', split_axis=0, concat_axis=0, tiled=True)  36.2 us
    dot_general x1, matrix products, per_device(): jnp.dot(hidden, lowering_matrices[0], preferred_element_type=jnp.float32)  26.5 us
    all_to_all x1, waiting for transfers between devices, per_device(): lax.all_to_all(payload, 'sp', split_axis=1, concat_axis=0, tiled=True)  17 us
    dot_general x1, matrix products, per_device(): jnp.dot(flattened, specialist_gating_matrices[0], preferred_element_type=...  13.8 us
    all_to_all x1, waiting for transfers between devices, per_device(): lax.all_to_all(outcome.astype(jnp.bfloat16), 'sp', split_axis=0, concat_a...  8.66 us
  transfers between devices with their start and end apart: 5, of which 5 were waited for; matrix products, arithmetic and copies ran while one was open for 1% of the time, Pallas kernels for 0%

commit v1 on v0

--- a/solution.py
+++ b/solution.py
@@ -1,7 +1,10 @@
 import jax
 import jax.numpy as jnp
 from jax import lax
+from jax.experimental import pallas as pl
+from jax.experimental.pallas import tpu as pltpu
 from jax.sharding import PartitionSpec as P
+
 
 HEADS = 16
 HEAD_DIM = 64
@@ -9,6 +12,7 @@
 STATE = 64
 KERNEL = 4
 BLK = 128
+CHUNKS = 2
 
 
 rms_eps = 1e-06
@@ -26,7 +30,7 @@
     return jax.nn.silu(running).astype(jnp.bfloat16)
 
 
-def ssd_blocks(x_conv, b_conv, c_conv, increment_delta, fading_exponent, init_state, block_len):
+def ssd_blocks(x_conv, b_conv, c_conv, increment_delta, fading_exponent, block_len):
     length, head_count, head_width = x_conv.shape
     state_width = b_conv.shape[2]
     block_count = length // block_len
@@ -59,9 +63,8 @@
     carry_weight = jnp.exp(
         jnp.where(earlier[:, :, None], before[:, None, :] - through[None, :, :], -jnp.inf)
     )
-    entering = (
-        jnp.einsum("cjh,jhpn->chpn", carry_weight, block_state, precision=lax.Precision.HIGHEST)
-        + jnp.exp(before)[:, :, None, None] * init_state[None]
+    entering = jnp.einsum(
+        "cjh,jhpn->chpn", carry_weight, block_state, precision=lax.Precision.HIGHEST
     )
     reach_decay = jnp.transpose(jnp.exp(cumulative), (0, 2, 1))
     carried_out = (
@@ -73,17 +76,229 @@
         )
         * reach_decay[:, :, :, None]
     )
-    outcome = (diag_out + carried_out).reshape(length, head_count, head_width)
-    final_state = (
-        jnp.einsum(
-            "jh,jhpn->hpn",
-            jnp.exp(through[-1][None, :] - through),
-            block_state,
-            precision=lax.Precision.HIGHEST,
-        )
-        + jnp.exp(through[-1])[:, None, None] * init_state
-    )
-    return (outcome, final_state, through[-1])
+    return (diag_out + carried_out).reshape(length, head_count, head_width)
+
+
+def join_kernel(*refs):
+    *block_refs, out_ref, sems = refs
+    count = block_refs[0].shape[0]
+    moves = [
+        pltpu.make_async_copy(block, out_ref.at[pl.ds(place * count, count)], sems.at[place])
+        for place, block in enumerate(block_refs)
+    ]
+    for move in moves:
+        move.start()
+    for move in moves:
+        move.wait()
+
+
+def join_rows(blocks):
+    count, width = blocks[0].shape
+    if count % 8:
+        return jnp.concatenate(blocks, axis=0)
+    return pl.pallas_call(
+        join_kernel,
+        in_specs=[pl.BlockSpec(memory_space=pl.ANY)] * len(blocks),
+        out_specs=pl.BlockSpec(memory_space=pltpu.HBM),
+        out_shape=jax.ShapeDtypeStruct((count * len(blocks), width), blocks[0].dtype),
+        scratch_shapes=[pltpu.SemaphoreType.DMA((len(blocks),))],
+        compiler_params=pltpu.CompilerParams(vmem_limit_bytes=1024 * 1024),
+        name="join_rows",
+    )(*blocks)
+
+
+def ffn_kernel(*refs):
+    count = (len(refs) - 10) // 2
+    pieces, (gate_hbm, up_hbm, down_hbm) = refs[:count], refs[count : count + 3]
+    outs = refs[count + 3 : 2 * count + 3]
+    rows, gate_ref, up_ref, down_ref, hidden_ref, stage, sems = refs[2 * count + 3 :]
+    size = pieces[0].shape[0]
+    width = rows.shape[1]
+    part = hidden_ref.shape[1]
+    out_tile = stage.shape[2]
+    tile = 256 if part % 256 == 0 else 128
+    first = part // tile
+    second = width // out_tile
+
+    def columns(place, extent):
+        return pl.ds(pl.multiple_of(place * extent, extent), extent)
+
+    def bring_piece(place):
+        spot = pl.ds(place * size, size)
+        return pltpu.make_async_copy(pieces[place], rows.at[spot], sems.at[0, place])
+
+    def bring_wide(place):
+        spot = columns(place, tile)
+        return (
+            pltpu.make_async_copy(gate_hbm.at[0, :, spot], gate_ref.at[:, spot], sems.at[1, place]),
+            pltpu.make_async_copy(up_hbm.at[0, :, spot], up_ref.at[:, spot], sems.at[2, place]),
+        )
+
+    def bring_down(place):
+        spot = columns(place, out_tile)
+        return pltpu.make_async_copy(
+            down_hbm.at[0, :, spot], down_ref.at[:, spot], sems.at[3, place]
+        )
+
+    def send(place, which):
+        return [
+            pltpu.make_async_copy(
+                stage.at[which, pl.ds(spot * size, size)],
+                out.at[:, columns(place, out_tile)],
+                sems.at[4 + which, spot],
+            )
+            for spot, out in enumerate(outs)
+        ]
+
+    def widen(block, place):
+        spot = columns(place, tile)
+        gate_val = jnp.dot(block, gate_ref[:, spot], preferred_element_type=jnp.float32)
+        up_val = jnp.dot(block, up_ref[:, spot], preferred_element_type=jnp.float32)
+        return (gate_val * jax.nn.sigmoid(gate_val) * up_val).astype(jnp.bfloat16)
+
+    for move in bring_wide(0):
+        move.start()
+    for place in range(count):
+        bring_piece(place).start()
+    for place in range(1, first):
+        for move in bring_wide(place):
+            move.start()
+    for place in range(second):
+        bring_down(place).start()
+
+    for move in bring_wide(0):
+        move.wait()
+    for place in range(count):
+        bring_piece(place).wait()
+        spot = pl.ds(place * size, size)
+        hidden_ref[spot, pl.ds(0, tile)] = widen(rows[spot, :], 0)
+
+    def wide_step(place, carry):
+        for move in bring_wide(place):
+            move.wait()
+        hidden_ref[:, columns(place, tile)] = widen(rows[...], place)
+        return carry
+
+    lax.fori_loop(1, first, wide_step, 0)
+
+    def down_step(place, carry):
+        which = lax.rem(place, 2)
+        bring_down(place).wait()
+        partial = jnp.dot(
+            hidden_ref[...], down_ref[:, columns(place, out_tile)], preferred_element_type=jnp.float32
+        )
+
+        @pl.when(place >= 2)
+        def _():
+            for move in send(place - 2, which):
+                move.wait()
+
+        stage[which] = partial.astype(jnp.bfloat16)
+        for move in send(place, which):
+            move.start()
+        return carry
+
+    lax.fori_loop(0, second, down_step, 0)
+    for place in range(max(second - 2, 0), second):
+        for move in send(place, place % 2):
+            move.wait()
+
+
+def expert_part(pieces, gate_w, up_w, down_w):
+    count, width = pieces[0].shape
+    total = count * len(pieces)
+    part = gate_w.shape[2]
+    out_tile = 512
+    hbm = pl.BlockSpec(memory_space=pltpu.HBM)
+    return pl.pallas_call(
+        ffn_kernel,
+        in_specs=[hbm] * (len(pieces) + 3),
+        out_specs=[hbm] * len(pieces),
+        out_shape=[jax.ShapeDtypeStruct((count, width), jnp.bfloat16)] * len(pieces),
+        scratch_shapes=[
+            pltpu.VMEM((total, width), jnp.bfloat16),
+            pltpu.VMEM((width, part), jnp.bfloat16),
+            pltpu.VMEM((width, part), jnp.bfloat16),
+            pltpu.VMEM((part, width), jnp.bfloat16),
+            pltpu.VMEM((total, part), jnp.bfloat16),
+            pltpu.VMEM((2, total, out_tile), jnp.bfloat16),
+            pltpu.SemaphoreType.DMA((6, max(len(pieces), part // 128, width // out_tile))),
+        ],
+        compiler_params=pltpu.CompilerParams(vmem_limit_bytes=36 * 1024 * 1024),
+        cost_estimate=pl.CostEstimate(
+            flops=total * width * part * 6,
+            transcendentals=total * part,
+            bytes_accessed=3 * width * part * 2 + 4 * total * width,
+        ),
+        name="expert_part",
+    )(*[pltpu.with_memory_space_constraint(v, pltpu.HBM) for v in (*pieces, gate_w, up_w, down_w)])
+
+
+def flip(value, mask):
+    size = lax.axis_size("dp")
+    return lax.ppermute(value, "dp", [(i, i ^ mask) for i in range(size)])
+
+
+def exchange(blocks):
+    size = lax.axis_size("sp")
+    arrived = [blocks[0]]
+    for gap in range(1, size):
+        arrived.append(lax.ppermute(blocks[gap], "sp", [(i, i ^ gap) for i in range(size)]))
+    return arrived
+
+
+def routed(normed, ids, shares, gate_w, up_w, down_w):
+    sp_size = lax.axis_size("sp")
+    dp_size = lax.axis_size("dp")
+    tok_rows, width = normed.shape
+    slot_cap = 3 * tok_rows // sp_size
+    flat_ids = ids.reshape(-1)
+    matched = (flat_ids[:, None] == jnp.arange(sp_size, dtype=jnp.int32)[None, :]).astype(jnp.int32)
+    ranked = jnp.cumsum(matched, axis=0) - 1
+    rank = jnp.sum(matched * ranked, axis=1).reshape(tok_rows, 2)
+    gaps = ids ^ lax.axis_index("sp").astype(jnp.int32)
+    span = slot_cap // CHUNKS
+    total = normed.astype(jnp.float32)
+    parts = []
+    for chunk in range(CHUNKS):
+        local = rank - chunk * span
+        inside = (local >= 0) & (local < span)
+        place = jnp.where(inside, gaps * span + local, -1)
+        slots = jnp.arange(sp_size * span, dtype=jnp.int32)
+        hit = slots[:, None, None] == place[None, :, :]
+        placing = jnp.sum(hit.astype(jnp.bfloat16), axis=2)
+        outgoing = (
+            jnp.dot(placing, normed, preferred_element_type=jnp.float32)
+            .astype(jnp.bfloat16)
+            .reshape(sp_size, span, width)
+        )
+        weight = jnp.sum(
+            jnp.where(place[:, :, None] == slots[None, None, :], shares[:, :, None], 0.0), axis=1
+        )
+        high = weight.astype(jnp.bfloat16)
+        low = (weight - high.astype(jnp.float32)).astype(jnp.bfloat16)
+        own = join_rows(exchange(outgoing))
+        parts.append((own, jnp.concatenate([high, low], axis=0)))
+    masks = [1 << bit for bit in range(1, dp_size.bit_length() - 1)] + [1]
+    for own, spread in parts:
+        pieces = [own]
+        for mask in masks:
+            pieces = pieces + [flip(piece, mask) for piece in pieces]
+        sums = [[value] for value in expert_part(pieces, gate_w, up_w, down_w)]
+        for mask in masks[::-1]:
+            half = len(sums) // 2
+            for place in range(half - 1, -1, -1):
+                leaving = sums[half + place]
+                sent = leaving[0]
+                if len(leaving) > 1:
+                    sent = sum(v.astype(jnp.float32) for v in leaving).astype(jnp.bfloat16)
+                sums[place].append(flip(sent, mask))
+            sums = sums[:half]
+        mine = sum(v.astype(jnp.float32) for v in sums[0]).astype(jnp.bfloat16)
+        answer = jnp.concatenate(exchange(mine.reshape(sp_size, span, width)), axis=0)
+        both = jnp.dot(spread, answer, preferred_element_type=jnp.float32)
+        total = total + both[:tok_rows] + both[tok_rows:]
+    return total.astype(jnp.bfloat16)
 
 
 def per_device(
@@ -111,7 +326,6 @@
     sp_size = lax.axis_size("sp")
     sp_index = lax.axis_index("sp")
     tok_rows = skip_connection_stream.shape[1]
-    model_width = skip_connection_stream.shape[2]
     inner_width = HEADS * HEAD_DIM
     per_group = HEADS // GROUPS
     paired = HEAD_DIM + 2 * STATE
@@ -144,14 +358,12 @@
     increment_delta = jax.nn.softplus(increment_premapped[0])
     speeds_per_channel = lax.dynamic_slice_in_dim(channel_fading_speed, first_head, head_count, 0)
     fading_exponent = extra_log_fading[0] - speeds_per_channel[None, :] * increment_delta
-    init_state = jnp.zeros((head_count, HEAD_DIM, STATE), jnp.float32)
-    outcome, final_state, total_decay = ssd_blocks(
+    outcome = ssd_blocks(
         convolved[:, :, :HEAD_DIM],
         convolved[:, :, HEAD_DIM : HEAD_DIM + STATE],
         convolved[:, :, HEAD_DIM + STATE :],
         increment_delta,
         fading_exponent,
-        init_state,
         BLK,
     )
     returned_rows = lax.all_to_all(
@@ -175,47 +387,14 @@
         (pre_norm - centre) * lax.rsqrt(variance + norm_eps) * standardize_scaling[None, :]
         + standardize_offset[None, :]
     ).astype(jnp.bfloat16)
-    slot_cap = 3 * tok_rows // sp_size
-    flat_ids = chosen_specialist_ids[0].reshape(-1)
-    matched = (flat_ids[:, None] == jnp.arange(sp_size, dtype=jnp.int32)[None, :]).astype(jnp.int32)
-    ranked = jnp.cumsum(matched, axis=0) - 1
-    target = flat_ids * slot_cap + jnp.sum(matched * ranked, axis=1)
-    placing = (jnp.arange(sp_size * slot_cap, dtype=jnp.int32)[:, None] == target[None, :]).astype(
-        jnp.bfloat16
-    )
-    placing = jnp.sum(placing.reshape(sp_size * slot_cap, tok_rows, 2), axis=2)
-    outgoing = (
-        jnp.dot(placing, normed, preferred_element_type=jnp.float32)
-        .astype(jnp.bfloat16)
-        .reshape(sp_size, slot_cap, model_width)
-    )
-    arrived_rows = lax.all_gather(
-        lax.all_to_all(outgoing, "sp", split_axis=0, concat_axis=0, tiled=True)[:, None],
-        "dp",
-        axis=1,
-        tiled=True,
-    )
-    flattened = arrived_rows.reshape(-1, model_width)
-    gate_val = jnp.dot(flattened, specialist_gating_matrices[0], preferred_element_type=jnp.float32)
-    up_val = jnp.dot(flattened, raising_matrices[0], preferred_element_type=jnp.float32)
-    hidden = (jax.nn.silu(gate_val) * up_val).astype(jnp.bfloat16)
-    partial_value = jnp.dot(
-        hidden, lowering_matrices[0], preferred_element_type=jnp.float32
-    ).astype(jnp.bfloat16)
-    partial_rows = (
-        lax.optimization_barrier(partial_value).astype(jnp.float32).reshape(arrived_rows.shape)
-    )
-    summed = lax.psum_scatter(
-        partial_rows.astype(jnp.bfloat16), "dp", scatter_dimension=1, tiled=True
-    )
-    item_count = partial_rows.shape[2]
-    answer_rows = summed.reshape(sp_size, item_count, model_width)
-    answered = lax.all_to_all(answer_rows, "sp", split_axis=0, concat_axis=0, tiled=True)
-    picked = answered.reshape(sp_size * slot_cap, model_width)[target.reshape(tok_rows, 2)]
-    routed_sum = jnp.sum(
-        specialist_mixing_shares[0][:, :, None] * picked.astype(jnp.float32), axis=1
-    )
-    layer_out = (normed.astype(jnp.float32) + routed_sum).astype(jnp.bfloat16)
+    layer_out = routed(
+        normed,
+        chosen_specialist_ids[0],
+        specialist_mixing_shares[0],
+        specialist_gating_matrices,
+        raising_matrices,
+        lowering_matrices,
+    )
     return layer_out[None]
 
 

time: 371 us -> 260 us (0.70)
  waiting for transfers between devices: 226 us -> 126 us
  starting transfers between devices: 16.8 us -> 68.2 us
  blocking collectives: 40.2 us -> 0 us
  matrix products: 46.4 us -> 7.07 us
  Pallas kernels: 0 us -> 37.2 us
  between operations: 13.9 us -> 0.77 us
  local copies, waits for them, and re-layouts: 17.3 us -> 10.7 us
    unnamed x3 -> x0, waiting for transfers between devices: 119 us -> none
    ppermute x0 -> x40, waiting for transfers between devices: none -> 101 us  [the longest x28 54.2 us: exchange(): lax.ppermute(blocks[gap], 'sp', [(i, i ^ gap) for i in range(size)])]
    ppermute x0 -> x40, starting transfers between devices: none -> 57.3 us  [the longest x28 51.9 us: exchange(): lax.ppermute(blocks[gap], 'sp', [(i, i ^ gap) for i in range(size)])]
    all_gather x1 -> x0, waiting for transfers between devices: 45.2 us -> none  [per_device(): lax.all_gather(lax.all_to_all(outgoing, 'sp', split_axis=0, concat_axis=0...]
    all_to_all x1 -> x0, blocking collectives: 40.2 us -> none  [per_device(): lax.all_to_all(outgoing, 'sp', split_axis=0, concat_axis=0, tiled=True)]
    dot_general x3 -> x4, matrix products: 41 us -> 1.62 us  [the longest x2 0.91 us: routed(): both = jnp.dot(spread, answer, preferred_element_type=jnp.float32)]
    pallas_call x0 -> x4, Pallas kernels: none -> 37.2 us  [the longest x2 35.1 us: expert_part(): pl.pallas_call(ffn_kernel, in_specs=[hbm] * (len(pieces) + 3), out_specs=...]
    all_to_all x1 -> x0, waiting for transfers between devices: 36.2 us -> none  [per_device(): lax.all_to_all(answer_rows, 'sp', split_axis=0, concat_axis=0, tiled=True)]
  transfers between devices with their start and end apart: 5 -> 42, of which waited for: 5 -> 24; matrix products, arithmetic and copies ran while one was open for 1% -> 2% of each run, Pallas kernels for 0% -> 14%
where the time goes in v1:
time: 260 us; the launch traced here: 259 us
  waiting for transfers between devices  126 us (48%)
  starting transfers between devices  68.2 us (26%)
  Pallas kernels  37.2 us (14%)
  local copies, waits for them, and re-layouts  10.7 us (4%)
  other arithmetic  8.64 us (3%)
  matrix products  7.07 us (3%)
    ppermute x28, waiting for transfers between devices, exchange(): lax.ppermute(blocks[gap], 'sp', [(i, i ^ gap) for i in range(size)])  54.2 us
    ppermute x28, starting transfers between devices, exchange(): lax.ppermute(blocks[gap], 'sp', [(i, i ^ gap) for i in range(size)])  51.9 us
    ppermute x12, waiting for transfers between devices, flip(): return lax.ppermute(value, 'dp', [(i, i ^ mask) for i in range(size)])  46.5 us
    pallas_call x2, Pallas kernels, expert_part(): pl.pallas_call(ffn_kernel, in_specs=[hbm] * (len(pieces) + 3), out_specs=...  35.1 us
    all_to_all x1, waiting for transfers between devices, per_device(): lax.all_to_all(payload, 'sp', split_axis=1, concat_axis=0, tiled=True)  17.3 us
    all_to_all x1, waiting for transfers between devices, per_device(): lax.all_to_all(outcome.astype(jnp.bfloat16), 'sp', split_axis=0, concat_a...  8.44 us
    unnamed x58, local copies, waits for them, and re-layouts  7.7 us
    all_to_all x1, starting transfers between devices, per_device(): lax.all_to_all(payload, 'sp', split_axis=1, concat_axis=0, tiled=True)  7.31 us
  transfers between devices with their start and end apart: 42, of which 24 were waited for; matrix products, arithmetic and copies ran while one was open for 2% of the time, Pallas kernels for 14%

profile of v1, /device:TPU:0, one launch (start us, length us, event | category | flops | bytes accessed | tf_op | source)
XLA Modules:
  0.0 259.1 jit_solution(8994728830080414816)
XLA Ops:
  4.2 7.3 %all-to-all-start = ((bf16[128,16,192]{0,2,1:T(8,128)(2,1)}), bf16[128,16,192]{0,2,1:T(8,128)(2,1)S(1)}, u32[]{:S(2)}, u32[]{:S(2)}) async-start(bf16[128,16,192]{0,2,1:T(8,128)(2,1)} %pad_maximum_fusion), calls=%async_computation | async-start | bytes 1572864 | tf_op jit(solution)/shard_map/all_to_all | solution.py:340
  14.4 17.3 %all-to-all-done = bf16[128,16,192]{0,2,1:T(8,128)(2,1)S(1)} async-done(((bf16[128,16,192]{0,2,1:T(8,128)(2,1)}), bf16[128,16,192]{0,2,1:T(8,128)(2,1)S(1)}, u32[]{:S(2)}, u32[]{:S(2)}) %all-to-all-start) | async-done | bytes 786464 | tf_op jit(solution)/shard_map/all_to_all | solution.py:340
  38.1 3.6 %all-to-all-start.1 = ((bf16[8,2,8192]{2,1,0:T(2,128)(2,1)}), bf16[8,2,8192]{2,1,0:T(2,128)(2,1)S(1)}, u32[]{:S(2)}, u32[]{:S(2)}) async-start(bf16[8,2,8192]{2,1,0:T(2,128)(2,1)} %reshape.311), calls=%async_computation.1 | async-start | bytes 524288 | tf_op jit(solution)/shard_map/all_to_all | solution.py:369
  42.3 8.4 %all-to-all-done.1 = bf16[8,2,8192]{2,1,0:T(2,128)(2,1)S(1)} async-done(((bf16[8,2,8192]{2,1,0:T(2,128)(2,1)}), bf16[8,2,8192]{2,1,0:T(2,128)(2,1)S(1)}, u32[]{:S(2)}, u32[]{:S(2)}) %all-to-all-start.1) | async-done | bytes 262176 | tf_op jit(solution)/shard_map/all_to_all | solution.py:369
  53.1 3.0 %fusion.80 = (f32[128]{0:T(128)S(1)}, f32[128,2048]{1,0:T(8,128)S(1)}) fusion(bf16[128,1024]{0,1:T(8,128)(2,1)S(1)} %fusion.14, bf16[1024,2048]{1,0:T(8,128)(2,1)} %param.32, bf16[1,128,2048]{2,1,0:T(8,128)(2,1)S(1)} %copy-done.2), kind=kOutput, calls=%fused_computation.162 | convolution fusion | flops 537657216 | bytes 6029824 | tf_op jit(solution)/shard_map/dot_general | solution.py:381
  61.9 3.0 %collective-permute-start.3 = (bf16[24,2048]{1,0:T(8,128)(2,1)S(1)}, bf16[24,2048]{1,0:T(8,128)(2,1)S(1)}, u32[]{:S(2)}, u32[]{:S(2)}) collective-permute-start(bf16[24,2048]{1,0:T(8,128)(2,1)S(1)} %get-tuple-element.38), channel_id=1, source_target_pairs={{0,16},{4,20},{8,24},{12,28},{16,0},{20,4},{24,8},{28,12},{1,17},{... | collective-permute-start | bytes 294920 | tf_op jit(solution)/shard_map/ppermute | solution.py:246
  65.6 6.6 %collective-permute-start.1 = (bf16[24,2048]{1,0:T(8,128)(2,1)S(1)}, bf16[24,2048]{1,0:T(8,128)(2,1)S(1)}, u32[]{:S(2)}, u32[]{:S(2)}) collective-permute-start(bf16[24,2048]{1,0:T(8,128)(2,1)S(1)} %get-tuple-element.40), channel_id=1, source_target_pairs={{0,8},{4,12},{8,0},{12,4},{16,24},{20,28},{24,16},{28,20},{1,9},{5... | collective-permute-start | bytes 294920 | tf_op jit(solution)/shard_map/ppermute | solution.py:246
  72.3 3.3 %collective-permute-done.4.refs_5_ = bf16[24,2048]{1,0:T(8,128)(2,1)S(1)} collective-permute-done((bf16[24,2048]{1,0:T(8,128)(2,1)S(1)}, bf16[24,2048]{1,0:T(8,128)(2,1)S(1)}, u32[]{:S(2)}, u32[]{:S(2)}) %collective-permute-start.4) | collective-permute-done | bytes 98336 | tf_op jit(solution)/shard_map/ppermute | solution.py:246
  83.9 3.7 %collective-permute-start.23 = (bf16[24,2048]{1,0:T(8,128)(2,1)S(1)}, bf16[24,2048]{1,0:T(8,128)(2,1)S(1)}, u32[]{:S(2)}, u32[]{:S(2)}) collective-permute-start(bf16[24,2048]{1,0:T(8,128)(2,1)S(1)} %get-tuple-element.54), channel_id=1, source_target_pairs={{0,16},{4,20},{8,24},{12,28},{16,0},{20,4},{24,8},{28,12},{1,17},{... | collective-permute-start | bytes 294920 | tf_op jit(solution)/shard_map/ppermute | solution.py:246
  87.6 7.9 %collective-permute-start.22 = (bf16[24,2048]{1,0:T(8,128)(2,1)S(1)}, bf16[24,2048]{1,0:T(8,128)(2,1)S(1)}, u32[]{:S(2)}, u32[]{:S(2)}) collective-permute-start(bf16[24,2048]{1,0:T(8,128)(2,1)S(1)} %get-tuple-element.55), channel_id=1, source_target_pairs={{0,12},{4,8},{8,4},{12,0},{16,28},{20,24},{24,20},{28,16},{1,13},{... | collective-permute-start | bytes 294920 | tf_op jit(solution)/shard_map/ppermute | solution.py:246
  104.2 14.4 %collective-permute-done.27.refs_1_ = bf16[192,2048]{1,0:T(8,128)(2,1)} collective-permute-done((bf16[192,2048]{1,0:T(8,128)(2,1)S(1)}, bf16[192,2048]{1,0:T(8,128)(2,1)}, u32[]{:S(2)}, u32[]{:S(2)}) %collective-permute-start.27) | collective-permute-done | bytes 786464 | tf_op jit(solution)/shard_map/ppermute | solution.py:239
  118.6 17.4 %expert_part.2 = (bf16[192,2048]{1,0:T(8,128)(2,1)S(1)}, bf16[192,2048]{1,0:T(8,128)(2,1)S(1)}, bf16[192,2048]{1,0:T(8,128)(2,1)S(1)}, bf16[192,2048]{1,0:T(8,128)(2,1)S(1)}) custom-call(bf16[192,2048]{1,0:T(8,128)(2,1)} %copy-done, bf16[192,2048]{1,0:T(8,128)(2,1)} %collective-permute-done.7.refs_1_, bf16[192,2048]{1,0:T(8,128)(2,1)} %collective-permute-done.8.refs_2_, ...), custom_call_target="tpu_custom_call" | custom-call | flops 12079595520 | bytes 22020096 | tf_op jit(solution)/shard_map/expert_part/pallas_call | solution.py:213
  138.4 17.6 %expert_part.3 = (bf16[192,2048]{1,0:T(8,128)(2,1)S(1)}, bf16[192,2048]{1,0:T(8,128)(2,1)S(1)}, bf16[192,2048]{1,0:T(8,128)(2,1)S(1)}, bf16[192,2048]{1,0:T(8,128)(2,1)S(1)}) custom-call(bf16[192,2048]{1,0:T(8,128)(2,1)} %copy-done.1, bf16[192,2048]{1,0:T(8,128)(2,1)} %collective-permute-done.27.refs_1_, bf16[192,2048]{1,0:T(8,128)(2,1)} %copy-done.15, ...), custom_call_target="tpu_custom_call" | custom-call | flops 12079595520 | bytes 22020096 | tf_op jit(solution)/shard_map/expert_part/pallas_call | solution.py:213
  159.6 17.9 %collective-permute-done.12 = bf16[192,2048]{1,0:T(8,128)(2,1)S(1)} collective-permute-done((bf16[192,2048]{1,0:T(8,128)(2,1)S(1)}, bf16[192,2048]{1,0:T(8,128)(2,1)S(1)}, u32[]{:S(2)}, u32[]{:S(2)}) %collective-permute-start.12) | collective-permute-done | bytes 786464 | tf_op jit(solution)/shard_map/ppermute | solution.py:239
  180.0 13.4 %collective-permute-done.32 = bf16[192,2048]{1,0:T(8,128)(2,1)S(1)} collective-permute-done((bf16[192,2048]{1,0:T(8,128)(2,1)S(1)}, bf16[192,2048]{1,0:T(8,128)(2,1)S(1)}, u32[]{:S(2)}, u32[]{:S(2)}) %collective-permute-start.32) | collective-permute-done | bytes 786464 | tf_op jit(solution)/shard_map/ppermute | solution.py:239
  201.6 5.8 %collective-permute-done.14 = bf16[24,2048]{1,0:T(8,128)(2,1)S(1)} collective-permute-done((bf16[24,2048]{1,0:T(8,128)(2,1)S(1)}, bf16[24,2048]{1,0:T(8,128)(2,1)S(1)}, u32[]{:S(2)}, u32[]{:S(2)}) %collective-permute-start.14) | collective-permute-done | bytes 98336 | tf_op jit(solution)/shard_map/ppermute | solution.py:246
  209.7 4.2 %collective-permute-done.15 = bf16[24,2048]{1,0:T(8,128)(2,1)S(1)} collective-permute-done((bf16[24,2048]{1,0:T(8,128)(2,1)S(1)}, bf16[24,2048]{1,0:T(8,128)(2,1)S(1)}, u32[]{:S(2)}, u32[]{:S(2)}) %collective-permute-start.15) | collective-permute-done | bytes 98336 | tf_op jit(solution)/shard_map/ppermute | solution.py:246
  215.7 5.2 %collective-permute-done.16 = bf16[24,2048]{1,0:T(8,128)(2,1)S(1)} collective-permute-done((bf16[24,2048]{1,0:T(8,128)(2,1)S(1)}, bf16[24,2048]{1,0:T(8,128)(2,1)S(1)}, u32[]{:S(2)}, u32[]{:S(2)}) %collective-permute-start.16) | collective-permute-done | bytes 98336 | tf_op jit(solution)/shard_map/ppermute | solution.py:246
  221.4 7.2 %collective-permute-done.17 = bf16[24,2048]{1,0:T(8,128)(2,1)S(1)} collective-permute-done((bf16[24,2048]{1,0:T(8,128)(2,1)S(1)}, bf16[24,2048]{1,0:T(8,128)(2,1)S(1)}, u32[]{:S(2)}, u32[]{:S(2)}) %collective-permute-start.17) | collective-permute-done | bytes 98336 | tf_op jit(solution)/shard_map/ppermute | solution.py:246
  229.8 5.2 %collective-permute-done.18 = bf16[24,2048]{1,0:T(8,128)(2,1)S(1)} collective-permute-done((bf16[24,2048]{1,0:T(8,128)(2,1)S(1)}, bf16[24,2048]{1,0:T(8,128)(2,1)S(1)}, u32[]{:S(2)}, u32[]{:S(2)}) %collective-permute-start.18) | collective-permute-done | bytes 98336 | tf_op jit(solution)/shard_map/ppermute | solution.py:246
  237.0 5.5 %collective-permute-done.19 = bf16[24,2048]{1,0:T(8,128)(2,1)S(1)} collective-permute-done((bf16[24,2048]{1,0:T(8,128)(2,1)S(1)}, bf16[24,2048]{1,0:T(8,128)(2,1)S(1)}, u32[]{:S(2)}, u32[]{:S(2)}) %collective-permute-start.19) | collective-permute-done | bytes 98336 | tf_op jit(solution)/shard_map/ppermute | solution.py:246
  243.4 3.6 %collective-permute-done.33 = bf16[24,2048]{1,0:T(8,128)(2,1)S(1)} collective-permute-done((bf16[24,2048]{1,0:T(8,128)(2,1)S(1)}, bf16[24,2048]{1,0:T(8,128)(2,1)S(1)}, u32[]{:S(2)}, u32[]{:S(2)}) %collective-permute-start.33) | collective-permute-done | bytes 98336 | tf_op jit(solution)/shard_map/ppermute | solution.py:246
  247.1 4.7 %collective-permute-done.34 = bf16[24,2048]{1,0:T(8,128)(2,1)S(1)} collective-permute-done((bf16[24,2048]{1,0:T(8,128)(2,1)S(1)}, bf16[24,2048]{1,0:T(8,128)(2,1)S(1)}, u32[]{:S(2)}, u32[]{:S(2)}) %collective-permute-start.34) | collective-permute-done | bytes 98336 | tf_op jit(solution)/shard_map/ppermute | solution.py:246
  252.4 4.9 %collective-permute-done.35 = bf16[24,2048]{1,0:T(8,128)(2,1)S(1)} collective-permute-done((bf16[24,2048]{1,0:T(8,128)(2,1)S(1)}, bf16[24,2048]{1,0:T(8,128)(2,1)S(1)}, u32[]{:S(2)}, u32[]{:S(2)}) %collective-permute-start.35) | collective-permute-done | bytes 98336 | tf_op jit(solution)/shard_map/ppermute | solution.py:246
  (206 shorter events, 67.4 us)
Async XLA Ops:
  4.2 27.5 %all-to-all-start = ((bf16[128,16,192]{0,2,1:T(8,128)(2,1)}), bf16[128,16,192]{0,2,1:T(8,128)(2,1)S(1)}, u32[]{:S(2)}, u32[]{:S(2)}) async-start(bf16[128,16,192]{0,2,1:T(8,128)(2,1)} %pad_maximum_fusion), calls=%async_computation | async-start | bytes 1572864 | tf_op jit(solution)/shard_map/all_to_all | solution.py:340
  38.1 12.7 %all-to-all-start.1 = ((bf16[8,2,8192]{2,1,0:T(2,128)(2,1)}), bf16[8,2,8192]{2,1,0:T(2,128)(2,1)S(1)}, u32[]{:S(2)}, u32[]{:S(2)}) async-start(bf16[8,2,8192]{2,1,0:T(2,128)(2,1)} %reshape.311), calls=%async_computation.1 | async-start | bytes 524288 | tf_op jit(solution)/shard_map/all_to_all | solution.py:369
  59.5 12.8 %collective-permute-start.5 = (bf16[24,2048]{1,0:T(8,128)(2,1)S(1)}, bf16[24,2048]{1,0:T(8,128)(2,1)S(1)}, u32[]{:S(2)}, u32[]{:S(2)}) collective-permute-start(bf16[24,2048]{1,0:T(8,128)(2,1)S(1)} %get-tuple-element.36), channel_id=1, source_target_pairs={{0,24},{4,28},{8,16},{12,20},{16,8},{20,12},{24,0},{28,4},{1,25},{... | collective-permute-start | bytes 294920 | tf_op jit(solution)/shard_map/ppermute | solution.py:246
  61.9 13.6 %collective-permute-start.4 = (bf16[24,2048]{1,0:T(8,128)(2,1)S(1)}, bf16[24,2048]{1,0:T(8,128)(2,1)S(1)}, u32[]{:S(2)}, u32[]{:S(2)}) collective-permute-start(bf16[24,2048]{1,0:T(8,128)(2,1)S(1)} %get-tuple-element.37), channel_id=1, source_target_pairs={{0,20},{4,16},{8,28},{12,24},{16,4},{20,0},{24,12},{28,8},{1,21},{... | collective-permute-start | bytes 294920 | tf_op jit(solution)/shard_map/ppermute | solution.py:246
  61.9 13.7 %collective-permute-start.3 = (bf16[24,2048]{1,0:T(8,128)(2,1)S(1)}, bf16[24,2048]{1,0:T(8,128)(2,1)S(1)}, u32[]{:S(2)}, u32[]{:S(2)}) collective-permute-start(bf16[24,2048]{1,0:T(8,128)(2,1)S(1)} %get-tuple-element.38), channel_id=1, source_target_pairs={{0,16},{4,20},{8,24},{12,28},{16,0},{20,4},{24,8},{28,12},{1,17},{... | collective-permute-start | bytes 294920 | tf_op jit(solution)/shard_map/ppermute | solution.py:246
  77.9 25.2 %collective-permute-start.7 = (bf16[192,2048]{1,0:T(8,128)(2,1)S(1)}, bf16[192,2048]{1,0:T(8,128)(2,1)}, u32[]{:S(2)}, u32[]{:S(2)}) collective-permute-start(bf16[192,2048]{1,0:T(8,128)(2,1)S(1)} %join_rows.2.refs_0_), channel_id=1, source_target_pairs={{0,2},{1,3},{2,0},{3,1},{4,6},{5,7},{6,4},{7,5},{8,10},{9,11},{10,... | collective-permute-start | bytes 2359304 | tf_op jit(solution)/shard_map/ppermute | solution.py:239
  82.0 13.5 %collective-permute-start.25 = (bf16[24,2048]{1,0:T(8,128)(2,1)S(1)}, bf16[24,2048]{1,0:T(8,128)(2,1)S(1)}, u32[]{:S(2)}, u32[]{:S(2)}) collective-permute-start(bf16[24,2048]{1,0:T(8,128)(2,1)S(1)} %get-tuple-element.52), channel_id=1, source_target_pairs={{0,24},{4,28},{8,16},{12,20},{16,8},{20,12},{24,0},{28,4},{1,25},{... | collective-permute-start | bytes 294920 | tf_op jit(solution)/shard_map/ppermute | solution.py:246
  83.6 13.2 %collective-permute-start.24 = (bf16[24,2048]{1,0:T(8,128)(2,1)S(1)}, bf16[24,2048]{1,0:T(8,128)(2,1)S(1)}, u32[]{:S(2)}, u32[]{:S(2)}) collective-permute-start(bf16[24,2048]{1,0:T(8,128)(2,1)S(1)} %get-tuple-element.53), channel_id=1, source_target_pairs={{0,20},{4,16},{8,28},{12,24},{16,4},{20,0},{24,12},{28,8},{1,21},{... | collective-permute-start | bytes 294920 | tf_op jit(solution)/shard_map/ppermute | solution.py:246
  83.9 14.9 %collective-permute-start.23 = (bf16[24,2048]{1,0:T(8,128)(2,1)S(1)}, bf16[24,2048]{1,0:T(8,128)(2,1)S(1)}, u32[]{:S(2)}, u32[]{:S(2)}) collective-permute-start(bf16[24,2048]{1,0:T(8,128)(2,1)S(1)} %get-tuple-element.54), channel_id=1, source_target_pairs={{0,16},{4,20},{8,24},{12,28},{16,0},{20,4},{24,8},{28,12},{1,17},{... | collective-permute-start | bytes 294920 | tf_op jit(solution)/shard_map/ppermute | solution.py:246
  87.6 11.3 %collective-permute-start.22 = (bf16[24,2048]{1,0:T(8,128)(2,1)S(1)}, bf16[24,2048]{1,0:T(8,128)(2,1)S(1)}, u32[]{:S(2)}, u32[]{:S(2)}) collective-permute-start(bf16[24,2048]{1,0:T(8,128)(2,1)S(1)} %get-tuple-element.55), channel_id=1, source_target_pairs={{0,12},{4,8},{8,4},{12,0},{16,28},{20,24},{24,20},{28,16},{1,13},{... | collective-permute-start | bytes 294920 | tf_op jit(solution)/shard_map/ppermute | solution.py:246
  102.6 16.1 %collective-permute-start.27 = (bf16[192,2048]{1,0:T(8,128)(2,1)S(1)}, bf16[192,2048]{1,0:T(8,128)(2,1)}, u32[]{:S(2)}, u32[]{:S(2)}) collective-permute-start(bf16[192,2048]{1,0:T(8,128)(2,1)S(1)} %join_rows.3.refs_0_), channel_id=1, source_target_pairs={{0,2},{1,3},{2,0},{3,1},{4,6},{5,7},{6,4},{7,5},{8,10},{9,11},{10,... | collective-permute-start | bytes 2359304 | tf_op jit(solution)/shard_map/ppermute | solution.py:239
  103.2 15.5 %collective-permute-start.8 = (bf16[192,2048]{1,0:T(8,128)(2,1)S(1)}, bf16[192,2048]{1,0:T(8,128)(2,1)}, u32[]{:S(2)}, u32[]{:S(2)}) collective-permute-start(bf16[192,2048]{1,0:T(8,128)(2,1)S(1)} %join_rows.2.refs_0_), channel_id=1, source_target_pairs={{0,1},{1,0},{2,3},{3,2},{4,5},{5,4},{6,7},{7,6},{8,9},{9,8},{10,11... | collective-permute-start | bytes 2359304 | tf_op jit(solution)/shard_map/ppermute | solution.py:239
  103.2 15.5 %collective-permute-start.9 = (bf16[192,2048]{1,0:T(8,128)(2,1)}, bf16[192,2048]{1,0:T(8,128)(2,1)}, u32[]{:S(2)}, u32[]{:S(2)}) collective-permute-start(bf16[192,2048]{1,0:T(8,128)(2,1)} %collective-permute-done.7.refs_1_), channel_id=1, source_target_pairs={{0,1},{1,0},{2,3},{3,2},{4,5},{5,4},{6,7},{7,6},{8,9},{9,8},{10,11... | collective-permute-start | bytes 2359304 | tf_op jit(solution)/shard_map/ppermute | solution.py:239
  104.1 32.6 %collective-permute-start.28 = (bf16[192,2048]{1,0:T(8,128)(2,1)S(1)}, bf16[192,2048]{1,0:T(8,128)(2,1)S(1)}, u32[]{:S(2)}, u32[]{:S(2)}) collective-permute-start(bf16[192,2048]{1,0:T(8,128)(2,1)S(1)} %join_rows.3.refs_0_), channel_id=1, source_target_pairs={{0,1},{1,0},{2,3},{3,2},{4,5},{5,4},{6,7},{7,6},{8,9},{9,8},{10,11... | collective-permute-start | bytes 2359304 | tf_op jit(solution)/shard_map/ppermute | solution.py:239
  118.6 18.0 %collective-permute-start.29 = (bf16[192,2048]{1,0:T(8,128)(2,1)}, bf16[192,2048]{1,0:T(8,128)(2,1)S(1)}, u32[]{:S(2)}, u32[]{:S(2)}) collective-permute-start(bf16[192,2048]{1,0:T(8,128)(2,1)} %collective-permute-done.27.refs_1_), channel_id=1, source_target_pairs={{0,1},{1,0},{2,3},{3,2},{4,5},{5,4},{6,7},{7,6},{8,9},{9,8},{10,11... | collective-permute-start | bytes 2359304 | tf_op jit(solution)/shard_map/ppermute | solution.py:239
  136.1 20.6 %collective-permute-start.11 = (bf16[192,2048]{1,0:T(8,128)(2,1)S(1)}, bf16[192,2048]{1,0:T(8,128)(2,1)S(1)}, u32[]{:S(2)}, u32[]{:S(2)}) collective-permute-start(bf16[192,2048]{1,0:T(8,128)(2,1)S(1)} %get-tuple-element.16), channel_id=1, source_target_pairs={{0,1},{1,0},{2,3},{3,2},{4,5},{5,4},{6,7},{7,6},{8,9},{9,8},{10,11... | collective-permute-start | bytes 2359304 | tf_op jit(solution)/shard_map/ppermute | solution.py:239
  156.9 20.5 %collective-permute-start.12 = (bf16[192,2048]{1,0:T(8,128)(2,1)S(1)}, bf16[192,2048]{1,0:T(8,128)(2,1)S(1)}, u32[]{:S(2)}, u32[]{:S(2)}) collective-permute-start(bf16[192,2048]{1,0:T(8,128)(2,1)S(1)} %add_convert_fusion.3), channel_id=1, source_target_pairs={{0,2},{1,3},{2,0},{3,1},{4,6},{5,7},{6,4},{7,5},{8,10},{9,11},{10,... | collective-permute-start | bytes 2359304 | tf_op jit(solution)/shard_map/ppermute | solution.py:239
  157.6 22.4 %collective-permute-start.30 = (bf16[192,2048]{1,0:T(8,128)(2,1)S(1)}, bf16[192,2048]{1,0:T(8,128)(2,1)S(1)}, u32[]{:S(2)}, u32[]{:S(2)}) collective-permute-start(bf16[192,2048]{1,0:T(8,128)(2,1)S(1)} %get-tuple-element.18), channel_id=1, source_target_pairs={{0,1},{1,0},{2,3},{3,2},{4,5},{5,4},{6,7},{7,6},{8,9},{9,8},{10,11... | collective-permute-start | bytes 2359304 | tf_op jit(solution)/shard_map/ppermute | solution.py:239
  158.7 34.7 %collective-permute-start.32 = (bf16[192,2048]{1,0:T(8,128)(2,1)S(1)}, bf16[192,2048]{1,0:T(8,128)(2,1)S(1)}, u32[]{:S(2)}, u32[]{:S(2)}) collective-permute-start(bf16[192,2048]{1,0:T(8,128)(2,1)S(1)} %add_convert_fusion.1), channel_id=1, source_target_pairs={{0,2},{1,3},{2,0},{3,1},{4,6},{5,7},{6,4},{7,5},{8,10},{9,11},{10,... | collective-permute-start | bytes 2359304 | tf_op jit(solution)/shard_map/ppermute | solution.py:239
  177.9 23.7 %collective-permute-start.13 = (bf16[24,2048]{1,0:T(8,128)(2,1)S(1)}, bf16[24,2048]{1,0:T(8,128)(2,1)S(1)}, u32[]{:S(2)}, u32[]{:S(2)}) collective-permute-start(bf16[24,2048]{1,0:T(8,128)(2,1)S(1)} %get-tuple-element.33), channel_id=1, source_target_pairs={{0,4},{4,0},{8,12},{12,8},{16,20},{20,16},{24,28},{28,24},{1,5},{5... | collective-permute-start | bytes 294920 | tf_op jit(solution)/shard_map/ppermute | solution.py:246
  193.9 63.5 %collective-permute-start.39 = (bf16[24,2048]{1,0:T(8,128)(2,1)S(1)}, bf16[24,2048]{1,0:T(8,128)(2,1)S(1)}, u32[]{:S(2)}, u32[]{:S(2)}) collective-permute-start(bf16[24,2048]{1,0:T(8,128)(2,1)S(1)} %get-tuple-element.43), channel_id=1, source_target_pairs={{0,28},{4,24},{8,20},{12,16},{16,12},{20,8},{24,4},{28,0},{1,29},{... | collective-permute-start | bytes 294920 | tf_op jit(solution)/shard_map/ppermute | solution.py:246
  196.8 60.5 %collective-permute-start.38 = (bf16[24,2048]{1,0:T(8,128)(2,1)S(1)}, bf16[24,2048]{1,0:T(8,128)(2,1)S(1)}, u32[]{:S(2)}, u32[]{:S(2)}) collective-permute-start(bf16[24,2048]{1,0:T(8,128)(2,1)S(1)} %get-tuple-element.44), channel_id=1, source_target_pairs={{0,24},{4,28},{8,16},{12,20},{16,8},{20,12},{24,0},{28,4},{1,25},{... | collective-permute-start | bytes 294920 | tf_op jit(solution)/shard_map/ppermute | solution.py:246
  199.2 58.1 %collective-permute-start.37 = (bf16[24,2048]{1,0:T(8,128)(2,1)S(1)}, bf16[24,2048]{1,0:T(8,128)(2,1)S(1)}, u32[]{:S(2)}, u32[]{:S(2)}) collective-permute-start(bf16[24,2048]{1,0:T(8,128)(2,1)S(1)} %get-tuple-element.45), channel_id=1, source_target_pairs={{0,20},{4,16},{8,28},{12,24},{16,4},{20,0},{24,12},{28,8},{1,21},{... | collective-permute-start | bytes 294920 | tf_op jit(solution)/shard_map/ppermute | solution.py:246
  199.2 58.0 %collective-permute-start.36 = (bf16[24,2048]{1,0:T(8,128)(2,1)S(1)}, bf16[24,2048]{1,0:T(8,128)(2,1)S(1)}, u32[]{:S(2)}, u32[]{:S(2)}) collective-permute-start(bf16[24,2048]{1,0:T(8,128)(2,1)S(1)} %get-tuple-element.46), channel_id=1, source_target_pairs={{0,16},{4,20},{8,24},{12,28},{16,0},{20,4},{24,8},{28,12},{1,17},{... | collective-permute-start | bytes 294920 | tf_op jit(solution)/shard_map/ppermute | solution.py:246
  (37 other events, 299.2 us)
